TPU v7x, 256 devices: a whole 4x4x8 slice. The times are simulated.
256 devices in a mesh: sp: 32 (over z, x), fs: 4 (over y), tp: 2 (over core).
Axes of the slice: x: 4, y: 4, z: 8, core: 2. Of those that a mesh axis runs over, the one named last changes fastest.
Arguments:
- inputs: bfloat16 [4, 8192, 2048], P('fs', ('sp', 'tp')), may hold values from -6 to 6
- norm_gain: float32 [2048], replicated, may hold values from 0.1 to 1.9
- w_glu_value: bfloat16 [2048, 1024], P(None, 'tp'), may hold values from -0.125 to 0.125
- w_glu_gate: bfloat16 [2048, 1024], P(None, 'tp'), may hold values from -0.125 to 0.125
- w_query_one: bfloat16 [2048, 512], P(None, 'tp'), may hold values from -2.5 to 2.5
- w_query_two: bfloat16 [2048, 512], P(None, 'tp'), may hold values from -2.5 to 2.5
- w_key_one: bfloat16 [2048, 512], P(None, 'tp'), may hold values from -2.5 to 2.5
- w_key_two: bfloat16 [2048, 512], P(None, 'tp'), may hold values from -2.5 to 2.5
- w_value: bfloat16 [2048, 1024], P(None, 'tp'), may hold values from -0.125 to 0.125
- conv_kernel: bfloat16 [31, 1024], P(None, 'tp'), may hold values from -1 to 1
- conv_gain: float32 [1024], P('tp'), may hold values from 0.1 to 1.9
- head_gain: float32 [128], replicated, may hold values from 0.1 to 1.9
- lambda_head: float32 [8], P('tp'), may hold values from 0.3 to 0.8
- w_out_conv: bfloat16 [1024, 2048], P('tp', 'fs'), may hold values from -0.125 to 0.125
- w_out_attn: bfloat16 [1024, 2048], P('tp', 'fs'), may hold values from -0.125 to 0.125
Outputs:
- mixed: bfloat16 [4, 8192, 2048], P('fs', ('sp', 'tp'))
- log_sums: float32 [4, 2, 8, 8192], P('fs', None, 'tp', 'sp')
All inputs are finite; a program needn't handle non-finite values.
Results may differ from a plain program's by a relative error of at most 0.013.
Values may be sent and summed in bfloat16 or wider, within the bound.
No kernel may reach another device: no remote copies, remote signals or barrier semaphores. Data moves between devices by JAX's collectives and lax.ppermute only.
A program may use at most 128 MiB of HBM per device.

v0:
```python
import functools

import jax
import jax.numpy as jnp
from jax import lax
from jax.experimental import pallas as pl
from jax.experimental.pallas import tpu as pltpu
from jax.sharding import Mesh, PartitionSpec as P


D = 2048
DC = 1024
HD = 64
VD = 128
CW = 31
SEG = 64
NZ, NX, NF, NT = 8, 4, 4, 2
BLOCK = 256
HALF = 128

NEG_FILL = -1e30
EPSILON = 1e-05
HEAD_SCALE = 0.8
LOG2E = 1.4426950408889634
LN2 = 0.6931471805599453


SWAP = [(0, 1), (1, 0)]
BF = jnp.bfloat16
F32 = jnp.float32


def head_route(step):
    return [
        (z * NT + t, (4 * t + (z + step) % 4) * NT + z // 4) for z in range(NZ) for t in range(NT)
    ]


def ring(count, step):
    return [(i, (i + step) % count) for i in range(count)]


def proj_kernel(
    own, peer, gain, wk1, wk2, wq1, wq2, wv, x_out, m0, m1, m2, m3, hk1, hk2, hq1, hq2, hv, packed, sems
):
    z, _, t = places()
    copies = [
        pltpu.make_async_copy(w, held, sems.at[i])
        for i, (w, held) in enumerate(
            ((wk1, hk1), (wk2, hk2), (wv, hv), (wq1, hq1), (wq2, hq2))
        )
    ]
    for copy in copies:
        copy.start()
    for place, rows in ((t, own), (1 - t, peer)):
        r = rows[...].astype(F32)
        scale = lax.rsqrt(jnp.mean(r * r, axis=-1, keepdims=True) + EPSILON)
        x_out[pl.ds(pl.multiple_of(place * HALF, HALF), HALF), :] = (r * scale * gain[...]).astype(
            BF
        )
    low = lax.broadcasted_iota(jnp.int32, (BLOCK, 2 * HD), 1) < HD

    def dot(held):
        return jnp.dot(x_out[...], held[...], preferred_element_type=F32).astype(BF).astype(F32)

    def both(a, b, head):
        pair = (head // 2) * 128
        a, b = a[:, pair : pair + 128], b[:, pair : pair + 128]
        if head % 2 == 0:
            return jnp.where(low, a, pltpu.roll(b, HD, 1))
        return jnp.where(low, pltpu.roll(a, HD, 1), b)

    def turned(value, head, column):
        for half in range(2):
            sl = slice(half * HALF, (half + 1) * HALF)
            packed[head, sl, column : column + 128] = value[sl].T.astype(BF)

    copies[0].wait()
    k1 = dot(hk1)
    copies[1].wait()
    k2 = dot(hk2)
    for head in range(4):
        packed[head, :, 0:128] = both(k1, k2, head).astype(BF)
    copies[2].wait()
    v = dot(hv)
    for head in range(4):
        turned(v[:, head * VD : (head + 1) * VD], head, 128)
    copies[3].wait()
    q1 = dot(hq1)
    copies[4].wait()
    q2 = dot(hq2)
    for head in range(4):
        turned(both(q1, q2, head) * (HD**-0.5), head, 256)
    for j, out in enumerate((m0, m1, m2, m3)):
        out[...] = packed[(z + j) % 4]


def project(own, peer, gain, wk1, wk2, wq1, wq2, wv):
    return pl.pallas_call(
        proj_kernel,
        in_specs=[VMEM] * 3 + [ANY] * 5,
        out_specs=[VMEM] * 5,
        out_shape=[jax.ShapeDtypeStruct((BLOCK, D), BF)]
        + [jax.ShapeDtypeStruct((BLOCK, 384), BF)] * 4,
        scratch_shapes=[pltpu.VMEM((D, 256), BF)] * 4
        + [
            pltpu.VMEM((D, 512), BF),
            pltpu.VMEM((4, BLOCK, 384), BF),
            pltpu.SemaphoreType.DMA((5,)),
        ],
        cost_estimate=pl.CostEstimate(
            flops=2 * BLOCK * D * 1536, transcendentals=0, bytes_accessed=8 * 2**20
        ),
        name="project",
    )(own, peer, gain, wk1, wk2, wq1, wq2, wv)


SMEM = pl.BlockSpec(memory_space=pltpu.SMEM)
VMEM = pl.BlockSpec(memory_space=pltpu.VMEM)
ANY = pl.BlockSpec(memory_space=pl.ANY)


def places():
    return tuple(lax.axis_index(a) for a in ("z", "x", "tp"))


def shard_copies(kv_a, kv_b, kv_s, sems, first=0):
    z, _, t = places()
    copies = []
    for j in range(kv_a.shape[0]):
        zz = (z + 4 - first - j) % 4
        for slot, kv in ((4 * t + zz, kv_a), (4 * (1 - t) + zz, kv_b)):
            sem = sems.at[2 * (first + j) + (kv is kv_b)]
            copies.append(pltpu.make_async_copy(kv.at[j], kv_s.at[slot], sem))
    return copies


def start(copies):
    for copy in copies:
        copy.start()


def wait(copies):
    for copy in copies:
        copy.wait()


def attend_shard(x2, kv_s, q_s, m_s, l_s, acc_s, before=None, after=None):
    _, x, t = places()
    key_seg = lax.broadcasted_iota(jnp.int32, (BLOCK, 256), 0) // SEG
    query_seg = (lax.broadcasted_iota(jnp.int32, (BLOCK, 256), 1) % HALF) // SEG
    allowed = key_seg - query_seg <= 2 * t + 8 * (x - x2)

    ones = jnp.ones((8, BLOCK), BF)

    def scores(zq):
        q = q_s[zq]
        parts = []
        for z2 in range(zq + 1):
            k = kv_s[z2, :, 0:128]
            s = jnp.dot(jnp.concatenate([k, k], axis=1), q, preferred_element_type=F32)
            if z2 == zq:
                s = jnp.where(allowed, s, NEG_FILL)
            parts.append(s)
        return parts

    def absorb(zq, parts):
        m_old = m_s[zq]
        top = None
        for s in parts:
            best = jnp.max(s.reshape(BLOCK // 8, 8, 256), axis=0)
            top = best if top is None else jnp.maximum(top, best)
        m_new = jnp.maximum(m_old, jnp.max(top, axis=0, keepdims=True))
        factor = jnp.exp2(m_old - m_new)
        weights = []
        values = []
        for z2, s in enumerate(parts):
            weights.append(jnp.exp2(s - m_new).astype(BF))
            vt = jnp.concatenate([kv_s[z2, 0:128, 128:256], kv_s[z2, 128:256, 128:256]], axis=1)
            values.append(jnp.concatenate([vt, ones], axis=0))
        pooled = jnp.dot(
            jnp.concatenate(values, axis=1),
            jnp.concatenate(weights, axis=0),
            preferred_element_type=F32,
        )
        m_s[zq] = m_new
        l_s[zq] = l_s[zq] * factor + pooled[128:129]
        acc_s[zq] = acc_s[zq] * factor + pooled[0:128]

    parts = scores(0)
    if before is not None:
        before()
    for zq in range(NZ):
        following = scores(zq + 1) if zq + 1 < NZ else None
        absorb(zq, parts)
        if after is not None:
            after(zq)
        parts = following


def state_copies(state, held, sems, inward):
    pairs = zip(state, held)
    return [
        pltpu.make_async_copy(*((a, b) if inward else (b, a)), sems.at[i])
        for i, (a, b) in enumerate(pairs)
    ]


def chunk_copy(acc_s, acc, sems, zq):
    return pltpu.make_async_copy(acc_s.at[zq], acc.at[zq], sems.at[zq])


def first_kernel(
    q_own, q_peer, kv_a, kv_b, q_out, m_out, l_out, acc_out, qt_s, q_s, m_s, l_s, acc_s, kv_s, sems, out_sems, aux
):
    z, x, t = places()
    queries = [
        pltpu.make_async_copy(q_own, qt_s.at[0], aux.at[0]),
        pltpu.make_async_copy(q_peer, qt_s.at[1], aux.at[1]),
    ]
    shard = shard_copies(kv_a, kv_b, kv_s, sems)
    start(queries)
    start(shard)
    m_s[...] = jnp.full(m_s.shape, NEG_FILL, F32)
    l_s[...] = jnp.zeros(l_s.shape, F32)
    acc_s[...] = jnp.zeros(acc_s.shape, F32)
    wait(queries)
    upper = lax.broadcasted_iota(jnp.int32, (128, HALF), 0) < HD
    for j in range(4):
        zz = (z + 4 - j) % 4
        for side, base in ((0, 4 * t), (1, 4 * (1 - t))):
            qt = qt_s[side, j].astype(F32) * LOG2E
            high = qt.astype(BF).astype(F32)
            for row, part in ((0, high), (128, qt - high)):
                q_s[base + zz, row : row + 128, 0:HALF] = jnp.where(upper, part, 0.0).astype(BF)
                q_s[base + zz, row : row + 128, HALF:256] = jnp.where(upper, 0.0, part).astype(BF)
    spread = pltpu.make_async_copy(q_s, q_out, aux.at[2])
    spread.start()
    wait(shard)
    chunks = [chunk_copy(acc_s, acc_out, out_sems, zq) for zq in range(NZ)]
    attend_shard(x, kv_s, q_s, m_s, l_s, acc_s, after=lambda zq: chunks[zq].start())
    ends = state_copies((m_out, l_out), (m_s, l_s), aux, False)
    start(ends)
    spread.wait()
    wait(chunks)
    wait(ends)


def middle_kernel(
    q_i,
    m_i,
    l_i,
    acc_i,
    kv_a,
    kv_b,
    kv_c,
    kv_d,
    m_out,
    l_out,
    acc_out,
    q_s,
    m_s,
    l_s,
    acc_s,
    kv_s,
    sems,
    out_sems,
    aux,
    *,
    steps,
):
    _, x, _ = places()
    queries = pltpu.make_async_copy(q_i, q_s, aux.at[3])
    first = shard_copies(kv_a, kv_b, kv_s.at[0], sems.at[0])
    state = state_copies((m_i, l_i, acc_i), (m_s, l_s, acc_s), aux, True)
    second = shard_copies(kv_c, kv_d, kv_s.at[1], sems.at[1])
    queries.start()
    start(first)
    start(state)
    start(second)
    queries.wait()
    wait(first)
    chunks = [chunk_copy(acc_s, acc_out, out_sems, zq) for zq in range(NZ)]

    @pl.loop(0, 2)
    def _(i):
        @pl.when(i == 0)
        def _():
            wait(state)

        @pl.when(i == 1)
        def _():
            wait(second)

        def after(zq):
            @pl.when(i == 1)
            def _():
                chunks[zq].start()

        x2 = (x + jnp.where(i == 0, steps[0], steps[1])) % 4
        attend_shard(x2, kv_s.at[i], q_s, m_s, l_s, acc_s, after=after)

    ends = state_copies((m_out, l_out), (m_s, l_s), aux, False)
    start(ends)
    wait(chunks)
    wait(ends)


def last_kernel(
    lam_a, lam_b, gain, q_s, m_i, l_i, acc_i, kv_a, kv_b, out, m_s, l_s, acc_s, kv_s, *, step
):
    z, x, t = places()
    m_s[...] = m_i[...]
    l_s[...] = l_i[...]
    acc_s[...] = acc_i[...]
    for j in range(4):
        zz = (z + 4 - j) % 4
        kv_s[4 * t + zz] = kv_a[j]
        kv_s[4 * (1 - t) + zz] = kv_b[j]
    attend_shard((x + step) % 4, kv_s, q_s, m_s, l_s, acc_s)
    lam_h = jnp.where(z // 4 == t, lam_a[z % 4], lam_b[z % 4])
    gain_row = gain[...] * HEAD_SCALE

    @pl.loop(0, NZ)
    def _(zq):
        denominator = l_s[zq]
        scaled = acc_s[zq] / denominator
        head = scaled[:, 0:HALF] - lam_h * scaled[:, HALF:256]
        square = jnp.mean(head * head, axis=0, keepdims=True)
        head = head * lax.rsqrt(square + EPSILON)
        out[zq, 0:HALF, :] = (head.T * gain_row).astype(BF)
        logs = m_s[zq] * LN2 + jnp.log(denominator)
        high = logs.astype(BF).astype(F32)
        rest = logs - high
        tail = jnp.concatenate(
            [
                high[:, 0:HALF],
                high[:, HALF:256],
                rest[:, 0:HALF],
                rest[:, HALF:256],
                jnp.zeros((4, HALF), F32),
            ],
            axis=0,
        )
        out[zq, HALF : HALF + 8, :] = tail.astype(BF)


STATE = [
    jax.ShapeDtypeStruct((NZ, 1, 256), F32),
    jax.ShapeDtypeStruct((NZ, 1, 256), F32),
    jax.ShapeDtypeStruct((NZ, 128, 256), F32),
]
HELD_STATE = [
    pltpu.VMEM((NZ, 1, 256), F32),
    pltpu.VMEM((NZ, 1, 256), F32),
    pltpu.VMEM((NZ, 128, 256), F32),
]
QUERIES = (NZ, 256, 256)
ATTEND_COST = pl.CostEstimate(
    flops=2 * 36 * BLOCK * 256 * 256, transcendentals=36 * BLOCK * 256, bytes_accessed=4 * 2**20
)


def dma(*shape):
    return pltpu.SemaphoreType.DMA(shape)


def attend_first(q_own, q_peer, kv_a, kv_b):
    return pl.pallas_call(
        first_kernel,
        in_specs=[ANY] * 4,
        out_specs=[ANY] * 4,
        out_shape=[jax.ShapeDtypeStruct(QUERIES, BF)] + STATE,
        scratch_shapes=[pltpu.VMEM((2, 4, 128, HALF), BF), pltpu.VMEM(QUERIES, BF)]
        + HELD_STATE
        + [pltpu.VMEM((NZ, BLOCK, 256), BF), dma(8), dma(NZ), dma(4)],
        cost_estimate=ATTEND_COST,
        name="attend_first",
    )(q_own, q_peer, kv_a, kv_b)


def attend_middle(q_s, state, kv, steps):
    return pl.pallas_call(
        functools.partial(middle_kernel, steps=steps),
        in_specs=[ANY] * 8,
        out_specs=[ANY] * 3,
        out_shape=STATE,
        scratch_shapes=[pltpu.VMEM(QUERIES, BF)]
        + HELD_STATE
        + [pltpu.VMEM((2, NZ, BLOCK, 256), BF), dma(2, 8), dma(NZ), dma(4)],
        cost_estimate=ATTEND_COST,
        name="attend_middle",
    )(q_s, *state, *kv)


def attend_last(lam_a, lam_b, gain, q_s, state, kv_a, kv_b, step):
    return pl.pallas_call(
        functools.partial(last_kernel, step=step),
        in_specs=[SMEM] * 2 + [VMEM] * 7,
        out_specs=VMEM,
        out_shape=jax.ShapeDtypeStruct((NZ, HALF + 8, 128), BF),
        scratch_shapes=HELD_STATE + [pltpu.VMEM((NZ, BLOCK, 256), BF)],
        cost_estimate=ATTEND_COST,
        name="attend_last",
    )(lam_a, lam_b, gain, q_s, *state, kv_a, kv_b)


def weight_copies(ws, held, sems):
    order = [i for d in range(4) for i in (d, 4 + d)]
    return [pltpu.make_async_copy(ws[i], held.at[i], sems.at[i]) for i in order]


def waited(ws, held, sems, d):
    for i in (d, 4 + d):
        pltpu.make_async_copy(ws[0], held.at[i], sems.at[i]).wait()


def conv_mix_kernel(c_own, c_peer, *refs):
    ws, out, held, sems = refs[:8], refs[8], refs[9], refs[10]
    start(weight_copies(ws, held, sems))

    @pl.loop(0, 4)
    def _(d):
        waited(ws, held, sems, d)
        out[d] = jnp.dot(c_own[...], held[d], preferred_element_type=F32) + jnp.dot(
            c_peer[...], held[4 + d], preferred_element_type=F32
        )


def final_kernel(heads, part, *refs):
    ws, out, held, sides, sems = refs[:8], refs[8], refs[9], refs[10], refs[11]
    y, t = lax.axis_index("fs"), lax.axis_index("tp")
    start(weight_copies(ws, held, sems))
    for side, base in ((0, 4 * t), (1, 4 * (1 - t))):
        for i in range(4):
            sides[side, :, i * VD : (i + 1) * VD] = heads[base + i, 0:HALF, :]

    @pl.loop(0, 4)
    def _(d):
        waited(ws, held, sems, d)
        mixed = (
            part[d]
            + jnp.dot(sides[0], held[d], preferred_element_type=F32)
            + jnp.dot(sides[1], held[4 + d], preferred_element_type=F32)
        )
        column = ((y + 4 - d) % 4) * 512
        out[:, pl.ds(pl.multiple_of(column, 512), 512)] = mixed.astype(BF)


MIX_COST = pl.CostEstimate(
    flops=2 * HALF * 1024 * 2048, transcendentals=0, bytes_accessed=6 * 2**20
)
MIX_WEIGHTS = pltpu.VMEM((8, 512, 512), BF)


def conv_mix(c_own, c_peer, ws):
    return pl.pallas_call(
        conv_mix_kernel,
        in_specs=[VMEM] * 2 + [ANY] * 8,
        out_specs=VMEM,
        out_shape=jax.ShapeDtypeStruct((4, HALF, 512), F32),
        scratch_shapes=[MIX_WEIGHTS, dma(8)],
        cost_estimate=MIX_COST,
        name="conv_mix",
    )(c_own, c_peer, *ws)


def final_mix(heads, part, ws):
    return pl.pallas_call(
        final_kernel,
        in_specs=[VMEM] * 2 + [ANY] * 8,
        out_specs=VMEM,
        out_shape=jax.ShapeDtypeStruct((HALF, D), BF),
        scratch_shapes=[MIX_WEIGHTS, pltpu.VMEM((2, HALF, 512), BF), dma(8)],
        cost_estimate=MIX_COST,
        name="final_mix",
    )(heads, part, *ws)


def body(
    inputs,
    norm_gain,
    w_glu_value,
    w_glu_gate,
    w_query_one,
    w_query_two,
    w_key_one,
    w_key_two,
    w_value,
    conv_kernel,
    conv_gain,
    head_gain,
    lambda_head,
    w_out_conv,
    w_out_attn,
):
    return layer(
        inputs,
        norm_gain,
        w_glu_value,
        w_glu_gate,
        (w_key_one, w_key_two, w_query_one, w_query_two, w_value),
        conv_kernel,
        conv_gain,
        head_gain,
        lambda_head,
        w_out_conv,
        w_out_attn,
    )


def swap(value):
    return lax.ppermute(value, "tp", SWAP)


def layer(
    inputs,
    norm_gain,
    w_glu_value,
    w_glu_gate,
    w_qkv,
    conv_kernel,
    conv_gain,
    head_gain,
    lambda_head,
    w_out_conv,
    w_out_attn,
):
    t = lax.axis_index("tp")

    own = inputs[0]
    peer = swap(own)
    normed, *messages = project(own, peer, norm_gain[None], *w_qkv)

    arrived = [lax.ppermute(m, ("z", "tp"), head_route(j)) for j, m in enumerate(messages)]
    kv = jnp.stack([m[:, 0:256] for m in arrived])
    queries = jnp.stack([m[:, 256:384] for m in arrived]).reshape(4, 2, HALF, 128)
    q_own = lax.dynamic_index_in_dim(queries, t, 1, keepdims=False)
    q_peer = swap(lax.dynamic_index_in_dim(queries, 1 - t, 1, keepdims=False))

    shards, swapped = {0: kv}, {0: swap(kv)}
    for step in (1, 3, 2):
        place = (-step) % 4
        shards[place] = lax.ppermute(kv, "x", ring(NX, step))
        swapped[place] = swap(shards[place])

    def gather_weight(w, far_step):
        near = {d: lax.ppermute(w, "fs", ring(NF, d)) for d in (1, 3)}
        far = lax.ppermute(near[far_step], "fs", ring(NF, far_step))
        sides = (w, near[1], far, near[3])
        return sides + tuple(swap(v) for v in sides)

    ws_conv = gather_weight(w_out_conv, 1)
    ws_attn = gather_weight(w_out_attn, 3)
    lambda_peer = swap(lambda_head)

    glu_value = jnp.dot(normed, w_glu_value, preferred_element_type=F32).astype(BF)
    glu_gate = jnp.dot(normed, w_glu_gate, preferred_element_type=F32).astype(BF)
    gated = (glu_value.astype(F32) * jax.nn.sigmoid(glu_gate.astype(F32))).astype(BF)
    count = NZ * NX
    earlier = lax.ppermute(
        gated[BLOCK - (CW - 1) :], ("z", "x"), [(i, i + 1) for i in range(count - 1)]
    )
    extended = jnp.concatenate([earlier, gated], axis=0).astype(F32)
    kernel_f = conv_kernel.astype(F32)
    convolved = jnp.zeros((BLOCK, 512), F32)
    for tap in range(CW):
        convolved = convolved + kernel_f[tap][None, :] * extended[tap : tap + BLOCK]
    sums = jnp.stack([jnp.sum(convolved, axis=-1), jnp.sum(convolved * convolved, axis=-1)])
    sums = sums + swap(sums)
    row_mean = (sums[0] / DC)[:, None]
    row_square = (sums[1] / DC)[:, None]
    conv_out = jax.nn.silu(
        (convolved - row_mean)
        * lax.rsqrt(row_square - row_mean * row_mean + EPSILON)
        * conv_gain
    ).astype(BF)
    conv_halves = conv_out.reshape(2, HALF, 512)
    conv_own = lax.dynamic_index_in_dim(conv_halves, t, 0, keepdims=False)
    conv_other = lax.dynamic_index_in_dim(conv_halves, 1 - t, 0, keepdims=False)
    conv_peer = swap(conv_other)
    part = conv_mix(conv_own, conv_peer, ws_conv)

    q_s, *state = attend_first(q_own, q_peer, shards[0], swapped[0])
    state = attend_middle(
        q_s, state, (shards[3], swapped[3], shards[1], swapped[1]), (3, 1)
    )
    returned = attend_last(
        lambda_head, lambda_peer, head_gain[None], q_s, state, shards[2], swapped[2], 2
    )

    heads = lax.all_to_all(returned, "z", 0, 0, tiled=True)
    mixed = final_mix(heads, part, ws_attn)

    tails = heads[:, HALF : HALF + 4, :].astype(F32)
    logs = (tails[:, 0:2] + tails[:, 2:4]).reshape(2, 4, 2, HALF)
    logs_own = lax.dynamic_index_in_dim(logs, t, 0, keepdims=False)
    logs_peer = swap(lax.dynamic_index_in_dim(logs, 1 - t, 0, keepdims=False))
    first = jnp.where(t == 0, logs_own, logs_peer)
    second = jnp.where(t == 0, logs_peer, logs_own)
    log_sums = jnp.transpose(jnp.concatenate([first, second], axis=-1), (1, 0, 2))
    return (mixed[None], log_sums[None])


def solution(mesh):
    grid = Mesh(mesh.devices.reshape(NZ, NX, NF, NT), ("z", "x", "fs", "tp"))
    weight = P(None, "tp")
    return jax.shard_map(
        body,
        mesh=grid,
        in_specs=(
            P("fs", ("z", "x", "tp"), None),
            P(),
            weight,
            weight,
            weight,
            weight,
            weight,
            weight,
            weight,
            weight,
            P("tp"),
            P(),
            P("tp"),
            P("tp", "fs"),
            P("tp", "fs"),
        ),
        out_specs=(P("fs", ("z", "x", "tp"), None), P("fs", None, "tp", ("z", "x"))),
        check_vma=False,
    )
```

profile of v0, /device:TPU:1, one launch (start us, length us, event | category | flops | bytes accessed | tf_op | source)
XLA Modules:
  0.0 141.1 jit_solution(13985406064839741463)
XLA Ops:
  0.6 3.3 %collective-permute-start.1 = (bf16[128,2048]{1,0:T(8,128)(2,1)}, bf16[128,2048]{1,0:T(8,128)(2,1)S(1)}, u32[]{:S(2)}, u32[]{:S(2)}) collective-permute-start(bf16[128,2048]{1,0:T(8,128)(2,1)} %bitcast.76), channel_id=1, source_target_pairs={{0,1},{1,0},{2,3},{3,2},{4,5},{5,4},{6,7},{7,6},{8,9},{9,8},{10,11... | collective-permute-start | bytes 1572872 | tf_op jit(solution)/shard_map/ppermute | solution.py:513
  3.9 2.7 %collective-permute-start.19 = (bf16[512,512]{1,0:T(8,128)(2,1)}, bf16[512,512]{1,0:T(8,128)(2,1)}, u32[]{:S(2)}, u32[]{:S(2)}) collective-permute-start(bf16[512,512]{1,0:T(8,128)(2,1)} %refs_0_.2), channel_id=1, source_target_pairs={{0,6},{2,0},{4,2},{6,4},{1,7},{3,1},{5,3},{7,5},{8,14},{10,8},{12,... | collective-permute-start | bytes 1572872 | tf_op jit(solution)/shard_map/ppermute | solution.py:548
  9.1 7.2 %project.1 = (bf16[256,2048]{1,0:T(8,128)(2,1)}, bf16[256,384]{1,0:T(8,128)(2,1)}, bf16[256,384]{1,0:T(8,128)(2,1)}, bf16[256,384]{1,0:T(8,128)(2,1)}, bf16[256,384]{1,0:T(8,128)(2,1)}) custom-call(bf16[128,2048]{1,0:T(8,128)(2,1)} %bitcast.77, bf16[128,2048]{1,0:T(8,128)(2,1)} %copy-done.6, f32[1,2048]{1,0:T(1,128)} %bitcast.121, bf16[2048,256]{1,0:T(8,128)(2,1)} %wk1.1, ...), custom_call_target="tpu_custom_call" | custom-call | flops 1610612736 | bytes 8388608 | tf_op jit(solution)/shard_map/project/pallas_call | solution.py:99
  16.3 3.8 %collective-permute-start.5 = (bf16[256,384]{1,0:T(8,128)(2,1)}, bf16[256,384]{1,0:T(8,128)(2,1)S(1)}, u32[]{:S(2)}, u32[]{:S(2)}) collective-permute-start(bf16[256,384]{1,0:T(8,128)(2,1)} %get-tuple-element.17), channel_id=1, source_target_pairs={{0,96},{1,224},{32,0},{33,128},{64,32},{65,160},{96,64},{97,192},{... | collective-permute-start | bytes 589832 | tf_op jit(solution)/shard_map/ppermute | solution.py:535
  20.2 2.2 %fusion.7 = f32[256,512]{1,0:T(8,128)S(1)} fusion(bf16[256,2048]{1,0:T(8,128)(2,1)} %get-tuple-element.25, bf16[2048,512]{1,0:T(8,128)(2,1)S(1)} %copy-done), kind=kOutput, calls=%fused_computation.9 | convolution fusion | flops 537526272 | bytes 3670016 | tf_op jit(solution)/shard_map/dot_general | solution.py:558
  23.1 3.1 %collective-permute-start.14 = (bf16[30,512]{1,0:T(8,128)(2,1)S(1)}, bf16[30,512]{1,0:T(8,128)(2,1)S(1)}, u32[]{:S(2)}, u32[]{:S(2)}) collective-permute-start(bf16[30,512]{1,0:T(8,128)(2,1)S(1)} %slice.313), channel_id=1, source_target_pairs={{0,8},{8,16},{16,24},{24,32},{32,40},{40,48},{48,56},{56,64},{64,7... | collective-permute-start | bytes 92168 | tf_op jit(solution)/shard_map/ppermute | solution.py:561
  27.3 10.8 %collective-permute-start.2 = (bf16[256,384]{1,0:T(8,128)(2,1)S(1)}, bf16[256,384]{1,0:T(8,128)(2,1)S(1)}, u32[]{:S(2)}, u32[]{:S(2)}) collective-permute-start(bf16[256,384]{1,0:T(8,128)(2,1)S(1)} %copy-done.14), channel_id=1, source_target_pairs={{0,0},{1,128},{32,32},{33,160},{64,64},{65,192},{96,96},{97,224},{... | collective-permute-start | bytes 589832 | tf_op jit(solution)/shard_map/ppermute | solution.py:535
  38.3 7.4 %collective-permute-done.4 = bf16[256,384]{1,0:T(8,128)(2,1)S(1)} collective-permute-done((bf16[256,384]{1,0:T(8,128)(2,1)S(1)}, bf16[256,384]{1,0:T(8,128)(2,1)S(1)}, u32[]{:S(2)}, u32[]{:S(2)}) %collective-permute-start.4) | collective-permute-done | bytes 196640 | tf_op jit(solution)/shard_map/ppermute | solution.py:535
  45.7 5.4 %collective-permute-start.3 = (bf16[256,384]{1,0:T(8,128)(2,1)S(1)}, bf16[256,384]{1,0:T(8,128)(2,1)S(1)}, u32[]{:S(2)}, u32[]{:S(2)}) collective-permute-start(bf16[256,384]{1,0:T(8,128)(2,1)S(1)} %copy-done.15), channel_id=1, source_target_pairs={{0,32},{1,160},{32,64},{33,192},{64,96},{65,224},{96,0},{97,128},{... | collective-permute-start | bytes 589832 | tf_op jit(solution)/shard_map/ppermute | solution.py:535
  51.1 4.7 %collective-permute-done.3 = bf16[256,384]{1,0:T(8,128)(2,1)S(1)} collective-permute-done((bf16[256,384]{1,0:T(8,128)(2,1)S(1)}, bf16[256,384]{1,0:T(8,128)(2,1)S(1)}, u32[]{:S(2)}, u32[]{:S(2)}) %collective-permute-start.3) | collective-permute-done | bytes 196640 | tf_op jit(solution)/shard_map/ppermute | solution.py:535
  57.3 2.6 %fusion.39 = (f32[256]{0:T(256)S(1)}, f32[256]{0:T(256)S(1)}, f32[256,512]{1,0:T(8,128)S(1)}) fusion(f32[286,512]{1,0:T(8,128)S(1)} %maximum_convert_fusion, f32[512]{0:T(512)S(1)} %bitcast.120, f32[512]{0:T(512)S(1)} %bitcast.119, f32[512]{0:T(512)S(1)} %bitcast.118, f32[512]{0:T(512)S(1)} %bitcast.117, f32[512]{0:T(512)S(1)} %bitcast.116, ...), kind=kLoop, calls=%fused_computation.97 | loop fusion | flops 8388096 | bytes 16842752 | tf_op jit(solution)/shard_map/reduce_sum | solution.py:569
  61.5 14.4 %collective-permute-done.10.kv_c = bf16[4,256,256]{2,1,0:T(8,128)(2,1)S(1)} collective-permute-done((bf16[4,256,256]{2,1,0:T(8,128)(2,1)S(1)}, bf16[4,256,256]{2,1,0:T(8,128)(2,1)S(1)}, u32[]{:S(2)}, u32[]{:S(2)}) %collective-permute-start.10) | collective-permute-done | bytes 524320 | tf_op jit(solution)/shard_map/ppermute | solution.py:544
  79.4 1.6 %collective-permute-start.25 = (bf16[512,512]{1,0:T(8,128)(2,1)S(1)}, bf16[512,512]{1,0:T(8,128)(2,1)}, u32[]{:S(2)}, u32[]{:S(2)}) collective-permute-start(bf16[512,512]{1,0:T(8,128)(2,1)S(1)} %copy-done.4), channel_id=1, source_target_pairs={{0,6},{2,0},{4,2},{6,4},{1,7},{3,1},{5,3},{7,5},{8,14},{10,8},{12,... | collective-permute-start | bytes 1572872 | tf_op jit(solution)/shard_map/ppermute | solution.py:548
  81.0 5.1 %collective-permute-done.8.kv_a = bf16[4,256,256]{2,1,0:T(8,128)(2,1)} collective-permute-done((bf16[4,256,256]{2,1,0:T(8,128)(2,1)S(1)}, bf16[4,256,256]{2,1,0:T(8,128)(2,1)}, u32[]{:S(2)}, u32[]{:S(2)}) %collective-permute-start.8) | collective-permute-done | bytes 524320 | tf_op jit(solution)/shard_map/ppermute | solution.py:544
  86.1 1.4 collective-permute-start.9
  88.3 5.5 %attend_first.1 = (bf16[8,256,256]{2,1,0:T(8,128)(2,1)}, f32[8,1,256]{2,1,0:T(1,128)}, f32[8,1,256]{2,1,0:T(1,128)}, f32[8,128,256]{2,1,0:T(8,128)}) custom-call(bf16[4,128,128]{2,1,0:T(8,128)(2,1)} %get-tuple-element.32.q_own, bf16[4,128,128]{2,1,0:T(8,128)(2,1)} %copy-done.17, bf16[4,256,256]{2,1,0:T(8,128)(2,1)} %copy-done.7, bf16[4,256,256]{2,1,0:T(8,128)(2,1)} %copy-done.12), custom_call_target="tpu_custom_call" | custom-call | flops 1207959552 | bytes 4194304 | tf_op jit(solution)/shard_map/attend_first/pallas_call | solution.py:369
  93.8 1.6 %collective-permute-start.24 = (bf16[512,512]{1,0:T(8,128)(2,1)S(1)}, bf16[512,512]{1,0:T(8,128)(2,1)}, u32[]{:S(2)}, u32[]{:S(2)}) collective-permute-start(bf16[512,512]{1,0:T(8,128)(2,1)S(1)} %copy-done.4), channel_id=1, source_target_pairs={{0,2},{2,4},{4,6},{6,0},{1,3},{3,5},{5,7},{7,1},{8,10},{10,12},{12... | collective-permute-start | bytes 1572872 | tf_op jit(solution)/shard_map/ppermute | solution.py:548
  95.4 9.7 %attend_middle.1 = (f32[8,1,256]{2,1,0:T(1,128)}, f32[8,1,256]{2,1,0:T(1,128)}, f32[8,128,256]{2,1,0:T(8,128)}) custom-call(bf16[8,256,256]{2,1,0:T(8,128)(2,1)} %get-tuple-element.18.q_i.q_s, f32[8,1,256]{2,1,0:T(1,128)} %get-tuple-element.19.m_i, f32[8,1,256]{2,1,0:T(1,128)} %get-tuple-element.20.l_i, f32[8,128,256]{2,1,0:T(8,128)} %get-tuple-element.21.acc_i, ...), custom_call_target="tpu_custom_call" | custom-call | flops 1207959552 | bytes 4194304 | tf_op jit(solution)/shard_map/attend_middle/pallas_call | solution.py:383
  105.8 1.4 collective-permute-start.26
  107.8 7.1 %attend_last.1 = bf16[8,136,128]{2,1,0:T(8,128)(2,1)} custom-call(f32[4]{0:T(128)} %lam_a.1, f32[4]{0:T(128)} %copy-done.18, f32[1,128]{1,0:T(1,128)} %bitcast.124, bf16[8,256,256]{2,1,0:T(8,128)(2,1)} %get-tuple-element.18.q_i.q_s, f32[8,1,256]{2,1,0:T(1,128)} %get-tuple-element.22.m_i, f32[8,1,256]{2,1,0:T(1,128)} %get-tuple-element.23.l_i, ...), custom_call_target="tpu_custom_call" | custom-call | flops 1207959552 | bytes 4194304 | tf_op jit(solution)/shard_map/attend_last/pallas_call | solution.py:397
  114.8 6.9 %all-to-all-start = ((bf16[8,136,128]{2,1,0:T(8,128)(2,1)}), bf16[8,136,128]{2,1,0:T(8,128)(2,1)S(1)}, u32[]{:S(2)}, u32[]{:S(2)}) async-start(bf16[8,136,128]{2,1,0:T(8,128)(2,1)} %attend_last.1), calls=%async_computation | async-start | bytes 557056 | tf_op jit(solution)/shard_map/all_to_all | solution.py:592
  125.0 4.5 %conv_mix.1.part = f32[4,128,512]{2,1,0:T(8,128)} custom-call(bf16[128,512]{1,0:T(8,128)(2,1)} %get-tuple-element.30.c_own, bf16[128,512]{1,0:T(8,128)(2,1)} %copy-done.8, bf16[512,512]{1,0:T(8,128)(2,1)} %refs_0_.2, bf16[512,512]{1,0:T(8,128)(2,1)} %collective-permute-done.17.refs_1_, bf16[512,512]{1,0:T(8,128)(2,1)} %collective-permute-done.18.refs_2_, ...), custom_call_target="tpu_custom_call" | custom-call | flops 536870912 | bytes 6291456 | tf_op jit(solution)/shard_map/conv_mix/pallas_call | solution.py:457
  129.6 4.9 %all-to-all-done.heads = bf16[8,136,128]{2,1,0:T(8,128)(2,1)S(1)} async-done(((bf16[8,136,128]{2,1,0:T(8,128)(2,1)}), bf16[8,136,128]{2,1,0:T(8,128)(2,1)S(1)}, u32[]{:S(2)}, u32[]{:S(2)}) %all-to-all-start) | async-done | bytes 278560 | tf_op jit(solution)/shard_map/all_to_all | solution.py:592
  135.8 4.6 %final_mix.1 = bf16[128,2048]{1,0:T(8,128)(2,1)} custom-call(bf16[8,136,128]{2,1,0:T(8,128)(2,1)} %copy-done.2, f32[4,128,512]{2,1,0:T(8,128)} %conv_mix.1.part, bf16[512,512]{1,0:T(8,128)(2,1)} %refs_0_.3, bf16[512,512]{1,0:T(8,128)(2,1)} %collective-permute-done.24.refs_1_, bf16[512,512]{1,0:T(8,128)(2,1)} %collective-permute-done.26.refs_2_, ...), custom_call_target="tpu_custom_call" | custom-call | flops 536870912 | bytes 6291456 | tf_op jit(solution)/shard_map/final_mix/pallas_call | solution.py:469
  (116 shorter events, 18.2 us)
Async XLA Ops:
  3.9 56.6 %collective-permute-start.17 = (bf16[512,512]{1,0:T(8,128)(2,1)}, bf16[512,512]{1,0:T(8,128)(2,1)}, u32[]{:S(2)}, u32[]{:S(2)}) collective-permute-start(bf16[512,512]{1,0:T(8,128)(2,1)} %refs_0_.2), channel_id=1, source_target_pairs={{0,2},{2,4},{4,6},{6,0},{1,3},{3,5},{5,7},{7,1},{8,10},{10,12},{12... | collective-permute-start | bytes 1572872 | tf_op jit(solution)/shard_map/ppermute | solution.py:548
  3.9 72.1 %collective-permute-start.19 = (bf16[512,512]{1,0:T(8,128)(2,1)}, bf16[512,512]{1,0:T(8,128)(2,1)}, u32[]{:S(2)}, u32[]{:S(2)}) collective-permute-start(bf16[512,512]{1,0:T(8,128)(2,1)} %refs_0_.2), channel_id=1, source_target_pairs={{0,6},{2,0},{4,2},{6,4},{1,7},{3,1},{5,3},{7,5},{8,14},{10,8},{12,... | collective-permute-start | bytes 1572872 | tf_op jit(solution)/shard_map/ppermute | solution.py:548
  6.6 53.3 %collective-permute-start = (f32[4]{0:T(128)}, f32[4]{0:T(128)S(1)}, u32[]{:S(2)}, u32[]{:S(2)}) collective-permute-start(f32[4]{0:T(128)} %lam_a.1), channel_id=1, source_target_pairs={{0,1},{1,0},{2,3},{3,2},{4,5},{5,4},{6,7},{7,6},{8,9},{9,8},{10,11... | collective-permute-start | bytes 56 | tf_op jit(solution)/shard_map/ppermute | solution.py:513
  16.3 21.8 %collective-permute-start.5 = (bf16[256,384]{1,0:T(8,128)(2,1)}, bf16[256,384]{1,0:T(8,128)(2,1)S(1)}, u32[]{:S(2)}, u32[]{:S(2)}) collective-permute-start(bf16[256,384]{1,0:T(8,128)(2,1)} %get-tuple-element.17), channel_id=1, source_target_pairs={{0,96},{1,224},{32,0},{33,128},{64,32},{65,160},{96,64},{97,192},{... | collective-permute-start | bytes 589832 | tf_op jit(solution)/shard_map/ppermute | solution.py:535
  27.3 28.6 %collective-permute-start.2 = (bf16[256,384]{1,0:T(8,128)(2,1)S(1)}, bf16[256,384]{1,0:T(8,128)(2,1)S(1)}, u32[]{:S(2)}, u32[]{:S(2)}) collective-permute-start(bf16[256,384]{1,0:T(8,128)(2,1)S(1)} %copy-done.14), channel_id=1, source_target_pairs={{0,0},{1,128},{32,32},{33,160},{64,64},{65,192},{96,96},{97,224},{... | collective-permute-start | bytes 589832 | tf_op jit(solution)/shard_map/ppermute | solution.py:535
  56.0 20.0 %collective-permute-start.10 = (bf16[4,256,256]{2,1,0:T(8,128)(2,1)S(1)}, bf16[4,256,256]{2,1,0:T(8,128)(2,1)S(1)}, u32[]{:S(2)}, u32[]{:S(2)}) collective-permute-start(bf16[4,256,256]{2,1,0:T(8,128)(2,1)S(1)} %pad_maximum_fusion.kv_a), channel_id=1, source_target_pairs={{0,24},{8,0},{16,8},{24,16},{1,25},{9,1},{17,9},{25,17},{2,26},{10... | collective-permute-start | bytes 1572872 | tf_op jit(solution)/shard_map/ppermute | solution.py:544
  59.8 19.5 %collective-permute-start.7 = (bf16[4,256,256]{2,1,0:T(8,128)(2,1)S(1)}, bf16[4,256,256]{2,1,0:T(8,128)(2,1)S(1)}, u32[]{:S(2)}, u32[]{:S(2)}) collective-permute-start(bf16[4,256,256]{2,1,0:T(8,128)(2,1)S(1)} %pad_maximum_fusion.kv_a), channel_id=1, source_target_pairs={{0,1},{1,0},{2,3},{3,2},{4,5},{5,4},{6,7},{7,6},{8,9},{9,8},{10,11... | collective-permute-start | bytes 1572872 | tf_op jit(solution)/shard_map/ppermute | solution.py:513
  60.0 26.1 %collective-permute-start.8 = (bf16[4,256,256]{2,1,0:T(8,128)(2,1)S(1)}, bf16[4,256,256]{2,1,0:T(8,128)(2,1)}, u32[]{:S(2)}, u32[]{:S(2)}) collective-permute-start(bf16[4,256,256]{2,1,0:T(8,128)(2,1)S(1)} %pad_maximum_fusion.kv_a), channel_id=1, source_target_pairs={{0,8},{8,16},{16,24},{24,0},{1,9},{9,17},{17,25},{25,1},{2,10},{10... | collective-permute-start | bytes 1572872 | tf_op jit(solution)/shard_map/ppermute | solution.py:544
  60.5 25.6 %collective-permute-start.12 = (bf16[4,256,256]{2,1,0:T(8,128)(2,1)S(1)}, bf16[4,256,256]{2,1,0:T(8,128)(2,1)}, u32[]{:S(2)}, u32[]{:S(2)}) collective-permute-start(bf16[4,256,256]{2,1,0:T(8,128)(2,1)S(1)} %pad_maximum_fusion.kv_a), channel_id=1, source_target_pairs={{0,16},{8,24},{16,0},{24,8},{1,17},{9,25},{17,1},{25,9},{2,18},{10... | collective-permute-start | bytes 1572872 | tf_op jit(solution)/shard_map/ppermute | solution.py:544
  75.9 11.5 %collective-permute-start.11 = (bf16[4,256,256]{2,1,0:T(8,128)(2,1)S(1)}, bf16[4,256,256]{2,1,0:T(8,128)(2,1)S(1)}, u32[]{:S(2)}, u32[]{:S(2)}) collective-permute-start(bf16[4,256,256]{2,1,0:T(8,128)(2,1)S(1)} %collective-permute-done.10.kv_c), channel_id=1, source_target_pairs={{0,1},{1,0},{2,3},{3,2},{4,5},{5,4},{6,7},{7,6},{8,9},{9,8},{10,11... | collective-permute-start | bytes 1572872 | tf_op jit(solution)/shard_map/ppermute | solution.py:513
  79.2 26.0 %collective-permute-start.20 = (bf16[512,512]{1,0:T(8,128)(2,1)}, bf16[512,512]{1,0:T(8,128)(2,1)}, u32[]{:S(2)}, u32[]{:S(2)}) collective-permute-start(bf16[512,512]{1,0:T(8,128)(2,1)} %refs_0_.2), channel_id=1, source_target_pairs={{0,1},{1,0},{2,3},{3,2},{4,5},{5,4},{6,7},{7,6},{8,9},{9,8},{10,11... | collective-permute-start | bytes 1572872 | tf_op jit(solution)/shard_map/ppermute | solution.py:513
  79.4 26.2 %collective-permute-start.25 = (bf16[512,512]{1,0:T(8,128)(2,1)S(1)}, bf16[512,512]{1,0:T(8,128)(2,1)}, u32[]{:S(2)}, u32[]{:S(2)}) collective-permute-start(bf16[512,512]{1,0:T(8,128)(2,1)S(1)} %copy-done.4), channel_id=1, source_target_pairs={{0,6},{2,0},{4,2},{6,4},{1,7},{3,1},{5,3},{7,5},{8,14},{10,8},{12,... | collective-permute-start | bytes 1572872 | tf_op jit(solution)/shard_map/ppermute | solution.py:548
  86.0 19.8 %collective-permute-start.18 = (bf16[512,512]{1,0:T(8,128)(2,1)}, bf16[512,512]{1,0:T(8,128)(2,1)}, u32[]{:S(2)}, u32[]{:S(2)}) collective-permute-start(bf16[512,512]{1,0:T(8,128)(2,1)} %collective-permute-done.17.refs_1_), channel_id=1, source_target_pairs={{0,2},{2,4},{4,6},{6,0},{1,3},{3,5},{5,7},{7,1},{8,10},{10,12},{12... | collective-permute-start | bytes 1572872 | tf_op jit(solution)/shard_map/ppermute | solution.py:549
  87.5 19.7 %collective-permute-start.13 = (bf16[4,256,256]{2,1,0:T(8,128)(2,1)}, bf16[4,256,256]{2,1,0:T(8,128)(2,1)}, u32[]{:S(2)}, u32[]{:S(2)}) collective-permute-start(bf16[4,256,256]{2,1,0:T(8,128)(2,1)} %collective-permute-done.12.kv_a), channel_id=1, source_target_pairs={{0,1},{1,0},{2,3},{3,2},{4,5},{5,4},{6,7},{7,6},{8,9},{9,8},{10,11... | collective-permute-start | bytes 1572872 | tf_op jit(solution)/shard_map/ppermute | solution.py:513
  93.8 28.8 %collective-permute-start.24 = (bf16[512,512]{1,0:T(8,128)(2,1)S(1)}, bf16[512,512]{1,0:T(8,128)(2,1)}, u32[]{:S(2)}, u32[]{:S(2)}) collective-permute-start(bf16[512,512]{1,0:T(8,128)(2,1)S(1)} %copy-done.4), channel_id=1, source_target_pairs={{0,2},{2,4},{4,6},{6,0},{1,3},{3,5},{5,7},{7,1},{8,10},{10,12},{12... | collective-permute-start | bytes 1572872 | tf_op jit(solution)/shard_map/ppermute | solution.py:548
  105.2 19.1 %collective-permute-start.21 = (bf16[512,512]{1,0:T(8,128)(2,1)}, bf16[512,512]{1,0:T(8,128)(2,1)}, u32[]{:S(2)}, u32[]{:S(2)}) collective-permute-start(bf16[512,512]{1,0:T(8,128)(2,1)} %collective-permute-done.17.refs_1_), channel_id=1, source_target_pairs={{0,1},{1,0},{2,3},{3,2},{4,5},{5,4},{6,7},{7,6},{8,9},{9,8},{10,11... | collective-permute-start | bytes 1572872 | tf_op jit(solution)/shard_map/ppermute | solution.py:513
  105.5 19.0 %collective-permute-start.23 = (bf16[512,512]{1,0:T(8,128)(2,1)}, bf16[512,512]{1,0:T(8,128)(2,1)}, u32[]{:S(2)}, u32[]{:S(2)}) collective-permute-start(bf16[512,512]{1,0:T(8,128)(2,1)} %collective-permute-done.19.refs_3_), channel_id=1, source_target_pairs={{0,1},{1,0},{2,3},{3,2},{4,5},{5,4},{6,7},{7,6},{8,9},{9,8},{10,11... | collective-permute-start | bytes 1572872 | tf_op jit(solution)/shard_map/ppermute | solution.py:513
  105.8 19.0 %collective-permute-start.26 = (bf16[512,512]{1,0:T(8,128)(2,1)}, bf16[512,512]{1,0:T(8,128)(2,1)}, u32[]{:S(2)}, u32[]{:S(2)}) collective-permute-start(bf16[512,512]{1,0:T(8,128)(2,1)} %collective-permute-done.25.refs_3_), channel_id=1, source_target_pairs={{0,6},{2,0},{4,2},{6,4},{1,7},{3,1},{5,3},{7,5},{8,14},{10,8},{12,... | collective-permute-start | bytes 1572872 | tf_op jit(solution)/shard_map/ppermute | solution.py:549
  107.2 17.9 %collective-permute-start.22 = (bf16[512,512]{1,0:T(8,128)(2,1)}, bf16[512,512]{1,0:T(8,128)(2,1)}, u32[]{:S(2)}, u32[]{:S(2)}) collective-permute-start(bf16[512,512]{1,0:T(8,128)(2,1)} %collective-permute-done.18.refs_2_), channel_id=1, source_target_pairs={{0,1},{1,0},{2,3},{3,2},{4,5},{5,4},{6,7},{7,6},{8,9},{9,8},{10,11... | collective-permute-start | bytes 1572872 | tf_op jit(solution)/shard_map/ppermute | solution.py:513
  114.8 19.6 %all-to-all-start = ((bf16[8,136,128]{2,1,0:T(8,128)(2,1)}), bf16[8,136,128]{2,1,0:T(8,128)(2,1)S(1)}, u32[]{:S(2)}, u32[]{:S(2)}) async-start(bf16[8,136,128]{2,1,0:T(8,128)(2,1)} %attend_last.1), calls=%async_computation | async-start | bytes 557056 | tf_op jit(solution)/shard_map/all_to_all | solution.py:592
  124.0 11.0 %collective-permute-start.27 = (bf16[512,512]{1,0:T(8,128)(2,1)S(1)}, bf16[512,512]{1,0:T(8,128)(2,1)S(1)}, u32[]{:S(2)}, u32[]{:S(2)}) collective-permute-start(bf16[512,512]{1,0:T(8,128)(2,1)S(1)} %copy-done.4), channel_id=1, source_target_pairs={{0,1},{1,0},{2,3},{3,2},{4,5},{5,4},{6,7},{7,6},{8,9},{9,8},{10,11... | collective-permute-start | bytes 1572872 | tf_op jit(solution)/shard_map/ppermute | solution.py:513
  124.3 10.8 %collective-permute-start.30 = (bf16[512,512]{1,0:T(8,128)(2,1)}, bf16[512,512]{1,0:T(8,128)(2,1)}, u32[]{:S(2)}, u32[]{:S(2)}) collective-permute-start(bf16[512,512]{1,0:T(8,128)(2,1)} %collective-permute-done.25.refs_3_), channel_id=1, source_target_pairs={{0,1},{1,0},{2,3},{3,2},{4,5},{5,4},{6,7},{7,6},{8,9},{9,8},{10,11... | collective-permute-start | bytes 1572872 | tf_op jit(solution)/shard_map/ppermute | solution.py:513
  124.5 10.5 %collective-permute-start.28 = (bf16[512,512]{1,0:T(8,128)(2,1)}, bf16[512,512]{1,0:T(8,128)(2,1)}, u32[]{:S(2)}, u32[]{:S(2)}) collective-permute-start(bf16[512,512]{1,0:T(8,128)(2,1)} %collective-permute-done.24.refs_1_), channel_id=1, source_target_pairs={{0,1},{1,0},{2,3},{3,2},{4,5},{5,4},{6,7},{7,6},{8,9},{9,8},{10,11... | collective-permute-start | bytes 1572872 | tf_op jit(solution)/shard_map/ppermute | solution.py:513
  124.8 10.3 %collective-permute-start.29 = (bf16[512,512]{1,0:T(8,128)(2,1)}, bf16[512,512]{1,0:T(8,128)(2,1)}, u32[]{:S(2)}, u32[]{:S(2)}) collective-permute-start(bf16[512,512]{1,0:T(8,128)(2,1)} %collective-permute-done.26.refs_2_), channel_id=1, source_target_pairs={{0,1},{1,0},{2,3},{3,2},{4,5},{5,4},{6,7},{7,6},{8,9},{9,8},{10,11... | collective-permute-start | bytes 1572872 | tf_op jit(solution)/shard_map/ppermute | solution.py:513
  (28 other events, 227.0 us)
where the time goes:
time: 142 us; the launch traced here: 141 us
  starting transfers between devices  49.8 us (35%)
  waiting for transfers between devices  40.3 us (28%)
  Pallas kernels  38.7 us (27%)
  local copies, waits for them, and re-layouts  4.78 us (3%)
  other arithmetic  3.64 us (3%)
  matrix products  2.86 us (2%)
    ppermute x4, starting transfers between devices, layer(): lax.ppermute(m, ('z', 'tp'), head_route(j))  20.2 us
    ppermute x3, waiting for transfers between devices, layer(): shards[place] = lax.ppermute(kv, 'x', ring(NX, step))  19.5 us
    ppermute x4, waiting for transfers between devices, layer(): lax.ppermute(m, ('z', 'tp'), head_route(j))  12.1 us
    pallas_call x1, Pallas kernels, attend_middle(): pl.pallas_call(functools.partial(middle_kernel, steps=steps), in_specs=[A...  9.72 us
    ppermute x18, starting transfers between devices, swap(): return lax.ppermute(value, 'tp', SWAP)  9.44 us
    pallas_call x1, Pallas kernels, project(): pl.pallas_call(proj_kernel, in_specs=[VMEM] * 3 + [ANY] * 5, out_specs=[V...  7.22 us
    pallas_call x1, Pallas kernels, attend_last(): pl.pallas_call(functools.partial(last_kernel, step=step), in_specs=[SMEM]...  7.06 us
    all_to_all x1, starting transfers between devices, layer(): heads = lax.all_to_all(returned, 'z', 0, 0, tiled=True)  6.87 us
  transfers between devices with their start and end apart: 33, of which 9 were waited for; matrix products, arithmetic and copies ran while one was open for 6% of the time, Pallas kernels for 27%

commit v1 on v0

--- a/solution.py
+++ b/solution.py
@@ -118,6 +118,66 @@
 SMEM = pl.BlockSpec(memory_space=pltpu.SMEM)
 VMEM = pl.BlockSpec(memory_space=pltpu.VMEM)
 ANY = pl.BlockSpec(memory_space=pl.ANY)
+
+
+def unpack_kernel(m0, m1, m2, m3, kv, q_own, q_other, held, in_sems, sems):
+    t = lax.axis_index("tp")
+    arrivals = [
+        pltpu.make_async_copy(m, held.at[j], in_sems.at[j]) for j, m in enumerate((m0, m1, m2, m3))
+    ]
+    start(arrivals)
+    copies = []
+    for j in range(4):
+        arrivals[j].wait()
+        mine = [pltpu.make_async_copy(held.at[j, :, pl.ds(0, 256)], kv.at[j], sems.at[j])]
+        for k, half, q in ((1, t, q_own), (2, 1 - t, q_other)):
+            rows = pl.ds(pl.multiple_of(half * HALF, HALF), HALF)
+            mine.append(
+                pltpu.make_async_copy(
+                    held.at[j, rows, pl.ds(256, 128)], q.at[j], sems.at[4 * k + j]
+                )
+            )
+        start(mine)
+        copies += mine
+    wait(copies)
+
+
+def unpack(arrived):
+    half = jax.ShapeDtypeStruct((4, HALF, 128), BF)
+    return pl.pallas_call(
+        unpack_kernel,
+        in_specs=[ANY] * 4,
+        out_specs=[ANY] * 3,
+        out_shape=[jax.ShapeDtypeStruct((4, BLOCK, 256), BF), half, half],
+        scratch_shapes=[pltpu.VMEM((4, BLOCK, 384), BF), dma(4), dma(12)],
+        name="unpack",
+    )(*arrived)
+
+
+def join_kernel(a, b, out, held, in_sems, sems):
+    inward = [
+        pltpu.make_async_copy(w, held.at[i], in_sems.at[i]) for i, w in enumerate((a, b))
+    ]
+    outward = [
+        pltpu.make_async_copy(held.at[i], out.at[pl.ds(512 * i, 512), :], sems.at[i])
+        for i in range(2)
+    ]
+    start(inward)
+    for i in range(2):
+        inward[i].wait()
+        outward[i].start()
+    wait(outward)
+
+
+def join(a, b):
+    return pl.pallas_call(
+        join_kernel,
+        in_specs=[ANY] * 2,
+        out_specs=ANY,
+        out_shape=jax.ShapeDtypeStruct((1024, 512), BF),
+        scratch_shapes=[pltpu.VMEM((2, 512, 512), BF), dma(2), dma(2)],
+        name="join",
+    )(a, b)
 
 
 def places():
@@ -321,7 +381,7 @@
     lam_h = jnp.where(z // 4 == t, lam_a[z % 4], lam_b[z % 4])
     gain_row = gain[...] * HEAD_SCALE
 
-    @pl.loop(0, NZ)
+    @pl.loop(0, NZ, unroll=8)
     def _(zq):
         denominator = l_s[zq]
         scaled = acc_s[zq] / denominator
@@ -405,19 +465,20 @@
     )(lam_a, lam_b, gain, q_s, *state, kv_a, kv_b)
 
 
-def weight_copies(ws, held, sems):
+def weight_copies(ws, held, sems, first):
     order = [i for d in range(4) for i in (d, 4 + d)]
-    return [pltpu.make_async_copy(ws[i], held.at[i], sems.at[i]) for i in order]
+    rows = pl.ds(first, 512)
+    return [pltpu.make_async_copy(ws[i].at[rows, :], held.at[i], sems.at[i]) for i in order]
 
 
 def waited(ws, held, sems, d):
     for i in (d, 4 + d):
-        pltpu.make_async_copy(ws[0], held.at[i], sems.at[i]).wait()
+        pltpu.make_async_copy(ws[0].at[pl.ds(0, 512), :], held.at[i], sems.at[i]).wait()
 
 
 def conv_mix_kernel(c_own, c_peer, *refs):
     ws, out, held, sems = refs[:8], refs[8], refs[9], refs[10]
-    start(weight_copies(ws, held, sems))
+    start(weight_copies(ws, held, sems, 0))
 
     @pl.loop(0, 4)
     def _(d):
@@ -427,13 +488,31 @@
         )
 
 
-def final_kernel(heads, part, *refs):
-    ws, out, held, sides, sems = refs[:8], refs[8], refs[9], refs[10], refs[11]
+def final_kernel(heads, part_i, *refs):
+    ws = refs[:8]
+    out, held, sides, part, out_s, sems, in_sems, out_sems = refs[8:]
     y, t = lax.axis_index("fs"), lax.axis_index("tp")
-    start(weight_copies(ws, held, sems))
-    for side, base in ((0, 4 * t), (1, 4 * (1 - t))):
-        for i in range(4):
-            sides[side, :, i * VD : (i + 1) * VD] = heads[base + i, 0:HALF, :]
+    rows = [
+        pltpu.make_async_copy(
+            heads.at[base + i, pl.ds(0, HALF), :],
+            sides.at[side, :, pl.ds(i * VD, VD)],
+            in_sems.at[4 * side + i],
+        )
+        for side, base in ((0, 4 * t), (1, 4 * (1 - t)))
+        for i in range(4)
+    ]
+    rows.append(pltpu.make_async_copy(part_i, part, in_sems.at[8]))
+    start(rows)
+    start(weight_copies(ws, held, sems, 512))
+    wait(rows)
+
+    def column(d):
+        return pl.ds(pl.multiple_of(((y + 4 - d) % 4) * 512, 512), 512)
+
+    def send(d):
+        return pltpu.make_async_copy(
+            out_s.at[:, column(d)], out.at[:, column(d)], out_sems.at[d]
+        )
 
     @pl.loop(0, 4)
     def _(d):
@@ -443,8 +522,11 @@
             + jnp.dot(sides[0], held[d], preferred_element_type=F32)
             + jnp.dot(sides[1], held[4 + d], preferred_element_type=F32)
         )
-        column = ((y + 4 - d) % 4) * 512
-        out[:, pl.ds(pl.multiple_of(column, 512), 512)] = mixed.astype(BF)
+        out_s[:, column(d)] = mixed.astype(BF)
+        send(d).start()
+
+    for d in range(4):
+        send(d).wait()
 
 
 MIX_COST = pl.CostEstimate(
@@ -468,10 +550,18 @@
 def final_mix(heads, part, ws):
     return pl.pallas_call(
         final_kernel,
-        in_specs=[VMEM] * 2 + [ANY] * 8,
-        out_specs=VMEM,
+        in_specs=[ANY] * 10,
+        out_specs=ANY,
         out_shape=jax.ShapeDtypeStruct((HALF, D), BF),
-        scratch_shapes=[MIX_WEIGHTS, pltpu.VMEM((2, HALF, 512), BF), dma(8)],
+        scratch_shapes=[
+            MIX_WEIGHTS,
+            pltpu.VMEM((2, HALF, 512), BF),
+            pltpu.VMEM((4, HALF, 512), F32),
+            pltpu.VMEM((HALF, D), BF),
+            dma(8),
+            dma(9),
+            dma(4),
+        ],
         cost_estimate=MIX_COST,
         name="final_mix",
     )(heads, part, *ws)
@@ -533,10 +623,8 @@
     normed, *messages = project(own, peer, norm_gain[None], *w_qkv)
 
     arrived = [lax.ppermute(m, ("z", "tp"), head_route(j)) for j, m in enumerate(messages)]
-    kv = jnp.stack([m[:, 0:256] for m in arrived])
-    queries = jnp.stack([m[:, 256:384] for m in arrived]).reshape(4, 2, HALF, 128)
-    q_own = lax.dynamic_index_in_dim(queries, t, 1, keepdims=False)
-    q_peer = swap(lax.dynamic_index_in_dim(queries, 1 - t, 1, keepdims=False))
+    kv, q_own, q_other = unpack(arrived)
+    q_peer = swap(q_other)
 
     shards, swapped = {0: kv}, {0: swap(kv)}
     for step in (1, 3, 2):
@@ -544,14 +632,9 @@
         shards[place] = lax.ppermute(kv, "x", ring(NX, step))
         swapped[place] = swap(shards[place])
 
-    def gather_weight(w, far_step):
-        near = {d: lax.ppermute(w, "fs", ring(NF, d)) for d in (1, 3)}
-        far = lax.ppermute(near[far_step], "fs", ring(NF, far_step))
-        sides = (w, near[1], far, near[3])
-        return sides + tuple(swap(v) for v in sides)
-
-    ws_conv = gather_weight(w_out_conv, 1)
-    ws_attn = gather_weight(w_out_attn, 3)
+    w_own = join(w_out_conv, w_out_attn)
+    w_sides = [w_own] + [lax.ppermute(w_own, "fs", ring(NF, d)) for d in (1, 2, 3)]
+    w_all = w_sides + [swap(w) for w in w_sides]
     lambda_peer = swap(lambda_head)
 
     glu_value = jnp.dot(normed, w_glu_value, preferred_element_type=F32).astype(BF)
@@ -579,7 +662,7 @@
     conv_own = lax.dynamic_index_in_dim(conv_halves, t, 0, keepdims=False)
     conv_other = lax.dynamic_index_in_dim(conv_halves, 1 - t, 0, keepdims=False)
     conv_peer = swap(conv_other)
-    part = conv_mix(conv_own, conv_peer, ws_conv)
+    part = conv_mix(conv_own, conv_peer, w_all)
 
     q_s, *state = attend_first(q_own, q_peer, shards[0], swapped[0])
     state = attend_middle(
@@ -590,7 +673,8 @@
     )
 
     heads = lax.all_to_all(returned, "z", 0, 0, tiled=True)
-    mixed = final_mix(heads, part, ws_attn)
+    heads, part = lax.optimization_barrier((heads, part))
+    mixed = final_mix(heads, part, w_all)
 
     tails = heads[:, HALF : HALF + 4, :].astype(F32)
     logs = (tails[:, 0:2] + tails[:, 2:4]).reshape(2, 4, 2, HALF)

time: 142 us -> 146 us (1.028)
  the two profiles are of different devices: /device:TPU:1 before, /device:TPU:17 now
where the time goes in v1:
time: 146 us; the launch traced here: 145 us
  starting transfers between devices  44.9 us (31%)
  waiting for transfers between devices  42.8 us (29%)
  Pallas kernels  41.7 us (29%)
  other arithmetic  6.92 us (5%)
  local copies, waits for them, and re-layouts  5.16 us (4%)
  matrix products  2.86 us (2%)
    ppermute x3, waiting for transfers between devices, layer(): lax.ppermute(w_own, 'fs', ring(NF, d))  28.3 us
    all_to_all x1, starting transfers between devices, layer(): heads = lax.all_to_all(returned, 'z', 0, 0, tiled=True)  16.9 us
    ppermute x4, starting transfers between devices, layer(): lax.ppermute(m, ('z', 'tp'), head_route(j))  13.5 us
    pallas_call x1, Pallas kernels, attend_middle(): pl.pallas_call(functools.partial(middle_kernel, steps=steps), in_specs=[A...  9.75 us
    pallas_call x1, Pallas kernels, project(): pl.pallas_call(proj_kernel, in_specs=[VMEM] * 3 + [ANY] * 5, out_specs=[V...  7.22 us
    ppermute x3, waiting for transfers between devices, layer(): shards[place] = lax.ppermute(kv, 'x', ring(NX, step))  6.78 us
    pallas_call x1, Pallas kernels, attend_last(): pl.pallas_call(functools.partial(last_kernel, step=step), in_specs=[SMEM]...  6.07 us
    pallas_call x1, Pallas kernels, attend_first(): pl.pallas_call(first_kernel, in_specs=[ANY] * 4, out_specs=[ANY] * 4, out...  5.56 us
  transfers between devices with their start and end apart: 26, of which 7 were waited for; matrix products, arithmetic and copies ran while one was open for 8% of the time, Pallas kernels for 24%

profile of v1, /device:TPU:17, one launch (start us, length us, event | category | flops | bytes accessed | tf_op | source)
XLA Modules:
  0.0 145.3 jit_solution(10829795062524099856)
XLA Ops:
  1.4 1.7 %fusion.41 = (f32[1,512]{1,0:T(1,128)S(1)}, f32[1,512]{1,0:T(1,128)S(1)}, f32[1,512]{1,0:T(1,128)S(1)}, f32[1,512]{1,0:T(1,128)S(1)}, f32[1,512]{1,0:T(1,128)}, ...) fusion(bf16[31,512]{1,0:T(8,128)(2,1)} %param.24), kind=kLoop, calls=%fused_computation.90 | loop fusion | bytes 77824 | tf_op jit(solution)/shard_map/slice | solution.py:651
  3.9 7.2 %project.1 = (bf16[256,2048]{1,0:T(8,128)(2,1)}, bf16[256,384]{1,0:T(8,128)(2,1)}, bf16[256,384]{1,0:T(8,128)(2,1)}, bf16[256,384]{1,0:T(8,128)(2,1)}, bf16[256,384]{1,0:T(8,128)(2,1)}) custom-call(bf16[128,2048]{1,0:T(8,128)(2,1)} %bitcast.61, bf16[128,2048]{1,0:T(8,128)(2,1)} %copy-done.5, f32[1,2048]{1,0:T(1,128)} %bitcast.101, bf16[2048,256]{1,0:T(8,128)(2,1)} %wk1.1, ...), custom_call_target="tpu_custom_call" | custom-call | flops 1610612736 | bytes 8388608 | tf_op jit(solution)/shard_map/project/pallas_call | solution.py:99
  11.2 9.1 %collective-permute-start.2 = (bf16[256,384]{1,0:T(8,128)(2,1)}, bf16[256,384]{1,0:T(8,128)(2,1)S(1)}, u32[]{:S(2)}, u32[]{:S(2)}) collective-permute-start(bf16[256,384]{1,0:T(8,128)(2,1)} %get-tuple-element.19), channel_id=1, source_target_pairs={{0,0},{1,128},{32,32},{33,160},{64,64},{65,192},{96,96},{97,224},{... | collective-permute-start | bytes 589832 | tf_op jit(solution)/shard_map/ppermute | solution.py:625
  20.3 4.3 %collective-permute-start.4 = (bf16[256,384]{1,0:T(8,128)(2,1)}, bf16[256,384]{1,0:T(8,128)(2,1)S(1)}, u32[]{:S(2)}, u32[]{:S(2)}) collective-permute-start(bf16[256,384]{1,0:T(8,128)(2,1)} %get-tuple-element.21), channel_id=1, source_target_pairs={{0,64},{1,192},{32,96},{33,224},{64,0},{65,128},{96,32},{97,160},{... | collective-permute-start | bytes 589832 | tf_op jit(solution)/shard_map/ppermute | solution.py:625
  24.7 2.2 %fusion.7 = f32[256,512]{1,0:T(8,128)S(1)} fusion(bf16[256,2048]{1,0:T(8,128)(2,1)} %get-tuple-element.33, bf16[2048,512]{1,0:T(8,128)(2,1)S(1)} %copy-done), kind=kOutput, calls=%fused_computation.9 | convolution fusion | flops 537526272 | bytes 3670016 | tf_op jit(solution)/shard_map/dot_general | solution.py:641
  27.6 3.1 %collective-permute-start.14 = (bf16[30,512]{1,0:T(8,128)(2,1)S(1)}, bf16[30,512]{1,0:T(8,128)(2,1)S(1)}, u32[]{:S(2)}, u32[]{:S(2)}) collective-permute-start(bf16[30,512]{1,0:T(8,128)(2,1)S(1)} %slice.273), channel_id=1, source_target_pairs={{0,8},{8,16},{16,24},{24,32},{32,40},{40,48},{48,56},{56,64},{64,7... | collective-permute-start | bytes 92168 | tf_op jit(solution)/shard_map/ppermute | solution.py:644
  31.4 2.1 %join.1.refs_0_ = bf16[1024,512]{1,0:T(8,128)(2,1)} custom-call(bf16[512,512]{1,0:T(8,128)(2,1)} %a.1, bf16[512,512]{1,0:T(8,128)(2,1)} %b.1), custom_call_target="tpu_custom_call" | custom-call | tf_op jit(solution)/shard_map/join/pallas_call | solution.py:173
  36.4 1.6 %collective-permute-done.5.m3 = bf16[256,384]{1,0:T(8,128)(2,1)} collective-permute-done((bf16[256,384]{1,0:T(8,128)(2,1)}, bf16[256,384]{1,0:T(8,128)(2,1)}, u32[]{:S(2)}, u32[]{:S(2)}) %collective-permute-start.5) | collective-permute-done | bytes 196640 | tf_op jit(solution)/shard_map/ppermute | solution.py:625
  38.1 2.0 %unpack.1 = (bf16[4,256,256]{2,1,0:T(8,128)(2,1)}, bf16[4,128,128]{2,1,0:T(8,128)(2,1)}, bf16[4,128,128]{2,1,0:T(8,128)(2,1)}) custom-call(bf16[256,384]{1,0:T(8,128)(2,1)} %copy-done.6, bf16[256,384]{1,0:T(8,128)(2,1)} %copy-done.7, bf16[256,384]{1,0:T(8,128)(2,1)} %copy-done.8, bf16[256,384]{1,0:T(8,128)(2,1)} %collective-permute-done.5.m3), custom_call_target="tpu_custom_call" | custom-call | tf_op jit(solution)/shard_map/unpack/pallas_call | solution.py:147
  40.2 4.2 %fusion.39 = (f32[256]{0:T(256)S(1)}, f32[256]{0:T(256)S(1)}, f32[256,512]{1,0:T(8,128)}) fusion(f32[286,512]{1,0:T(8,128)S(1)} %maximum_convert_fusion, f32[512]{0:T(512)} %bitcast.100, f32[512]{0:T(512)} %bitcast.99, f32[512]{0:T(512)} %bitcast.98, f32[512]{0:T(512)} %bitcast.97, f32[512]{0:T(512)} %bitcast.96, f32[512]{0:T(512)} %bitcast.95, ...), kind=kLoop, calls=%fused_computation.89 | loop fusion | flops 8388096 | bytes 16842752 | tf_op jit(solution)/shard_map/reduce_sum | solution.py:652
  46.2 1.2 collective-permute-start.8
  47.4 1.5 %collective-permute-start.10 = (bf16[4,256,256]{2,1,0:T(8,128)(2,1)}, bf16[4,256,256]{2,1,0:T(8,128)(2,1)}, u32[]{:S(2)}, u32[]{:S(2)}) collective-permute-start(bf16[4,256,256]{2,1,0:T(8,128)(2,1)} %get-tuple-element.25.kv_a), channel_id=1, source_target_pairs={{0,24},{8,0},{16,8},{24,16},{1,25},{9,1},{17,9},{25,17},{2,26},{10... | collective-permute-start | bytes 1572872 | tf_op jit(solution)/shard_map/ppermute | solution.py:632
  48.9 28.3 %collective-permute-done.17.refs_1_ = bf16[1024,512]{1,0:T(8,128)(2,1)} collective-permute-done((bf16[1024,512]{1,0:T(8,128)(2,1)}, bf16[1024,512]{1,0:T(8,128)(2,1)}, u32[]{:S(2)}, u32[]{:S(2)}) %collective-permute-start.17) | collective-permute-done | bytes 1048608 | tf_op jit(solution)/shard_map/ppermute | solution.py:636
  77.2 2.5 %collective-permute-start.12 = (bf16[4,256,256]{2,1,0:T(8,128)(2,1)}, bf16[4,256,256]{2,1,0:T(8,128)(2,1)}, u32[]{:S(2)}, u32[]{:S(2)}) collective-permute-start(bf16[4,256,256]{2,1,0:T(8,128)(2,1)} %get-tuple-element.25.kv_a), channel_id=1, source_target_pairs={{0,16},{8,24},{16,0},{24,8},{1,17},{9,25},{17,1},{25,9},{2,18},{10... | collective-permute-start | bytes 1572872 | tf_op jit(solution)/shard_map/ppermute | solution.py:632
  80.2 6.8 %collective-permute-done.12.kv_a = bf16[4,256,256]{2,1,0:T(8,128)(2,1)} collective-permute-done((bf16[4,256,256]{2,1,0:T(8,128)(2,1)}, bf16[4,256,256]{2,1,0:T(8,128)(2,1)}, u32[]{:S(2)}, u32[]{:S(2)}) %collective-permute-start.12) | collective-permute-done | bytes 524320 | tf_op jit(solution)/shard_map/ppermute | solution.py:632
  88.5 5.6 %attend_first.1 = (bf16[8,256,256]{2,1,0:T(8,128)(2,1)}, f32[8,1,256]{2,1,0:T(1,128)}, f32[8,1,256]{2,1,0:T(1,128)}, f32[8,128,256]{2,1,0:T(8,128)}) custom-call(bf16[4,128,128]{2,1,0:T(8,128)(2,1)} %get-tuple-element.23.q_own, bf16[4,128,128]{2,1,0:T(8,128)(2,1)} %copy-done.13, bf16[4,256,256]{2,1,0:T(8,128)(2,1)} %get-tuple-element.25.kv_a, ...), custom_call_target="tpu_custom_call" | custom-call | flops 1207959552 | bytes 4194304 | tf_op jit(solution)/shard_map/attend_first/pallas_call | solution.py:429
  94.1 9.7 %attend_middle.1 = (f32[8,1,256]{2,1,0:T(1,128)}, f32[8,1,256]{2,1,0:T(1,128)}, f32[8,128,256]{2,1,0:T(8,128)}) custom-call(bf16[8,256,256]{2,1,0:T(8,128)(2,1)} %get-tuple-element.26.q_i.q_s, f32[8,1,256]{2,1,0:T(1,128)} %get-tuple-element.27.m_i, f32[8,1,256]{2,1,0:T(1,128)} %get-tuple-element.28.l_i, f32[8,128,256]{2,1,0:T(8,128)} %get-tuple-element.29.acc_i, ...), custom_call_target="tpu_custom_call" | custom-call | flops 1207959552 | bytes 4194304 | tf_op jit(solution)/shard_map/attend_middle/pallas_call | solution.py:443
  103.8 6.1 %attend_last.1 = bf16[8,136,128]{2,1,0:T(8,128)(2,1)} custom-call(f32[4]{0:T(128)} %lam_a.1, f32[4]{0:T(128)} %copy-done.15, f32[1,128]{1,0:T(1,128)} %bitcast.104, bf16[8,256,256]{2,1,0:T(8,128)(2,1)} %get-tuple-element.26.q_i.q_s, f32[8,1,256]{2,1,0:T(1,128)} %get-tuple-element.30.m_i, f32[8,1,256]{2,1,0:T(1,128)} %get-tuple-element.31.l_i, ...), custom_call_target="tpu_custom_call" | custom-call | flops 1207959552 | bytes 4194304 | tf_op jit(solution)/shard_map/attend_last/pallas_call | solution.py:457
  109.9 16.9 %all-to-all-start = ((bf16[8,136,128]{2,1,0:T(8,128)(2,1)}), bf16[8,136,128]{2,1,0:T(8,128)(2,1)S(1)}, u32[]{:S(2)}, u32[]{:S(2)}) async-start(bf16[8,136,128]{2,1,0:T(8,128)(2,1)} %attend_last.1), calls=%async_computation | async-start | bytes 557056 | tf_op jit(solution)/shard_map/all_to_all | solution.py:675
  126.9 1.3 multiply_convert_fusion
  129.4 1.2 collective-permute-done.16.c_peer
  131.2 4.5 %conv_mix.1.part_i = f32[4,128,512]{2,1,0:T(8,128)} custom-call(bf16[128,512]{1,0:T(8,128)(2,1)} %get-tuple-element.40.c_own, bf16[128,512]{1,0:T(8,128)(2,1)} %copy-done.9, bf16[1024,512]{1,0:T(8,128)(2,1)} %join.1.refs_0_, bf16[1024,512]{1,0:T(8,128)(2,1)} %collective-permute-done.17.refs_1_, bf16[1024,512]{1,0:T(8,128)(2,1)} %collective-permute-done.18.refs_2_, ...), custom_call_target="tpu_custom_call" | custom-call | flops 536870912 | bytes 6291456 | tf_op jit(solution)/shard_map/conv_mix/pallas_call | solution.py:539
  135.7 3.7 %all-to-all-done.heads = bf16[8,136,128]{2,1,0:T(8,128)(2,1)S(1)} async-done(((bf16[8,136,128]{2,1,0:T(8,128)(2,1)}), bf16[8,136,128]{2,1,0:T(8,128)(2,1)S(1)}, u32[]{:S(2)}, u32[]{:S(2)}) %all-to-all-start) | async-done | bytes 278560 | tf_op jit(solution)/shard_map/all_to_all | solution.py:675
  140.2 4.5 %final_mix.1 = bf16[128,2048]{1,0:T(8,128)(2,1)} custom-call(bf16[8,136,128]{2,1,0:T(8,128)(2,1)} %copy-done.3, f32[4,128,512]{2,1,0:T(8,128)} %conv_mix.1.part_i, bf16[1024,512]{1,0:T(8,128)(2,1)} %join.1.refs_0_, bf16[1024,512]{1,0:T(8,128)(2,1)} %collective-permute-done.17.refs_1_, bf16[1024,512]{1,0:T(8,128)(2,1)} %collective-permute-done.18.refs_2_, ...), custom_call_target="tpu_custom_call" | custom-call | flops 536870912 | bytes 6291456 | tf_op jit(solution)/shard_map/final_mix/pallas_call | solution.py:551
  (87 shorter events, 13.2 us)
Async XLA Ops:
  0.6 2.5 %collective-permute-start.1 = (bf16[128,2048]{1,0:T(8,128)(2,1)}, bf16[128,2048]{1,0:T(8,128)(2,1)S(1)}, u32[]{:S(2)}, u32[]{:S(2)}) collective-permute-start(bf16[128,2048]{1,0:T(8,128)(2,1)} %bitcast.60), channel_id=1, source_target_pairs={{0,1},{1,0},{2,3},{3,2},{4,5},{5,4},{6,7},{7,6},{8,9},{9,8},{10,11... | collective-permute-start | bytes 1572872 | tf_op jit(solution)/shard_map/ppermute | solution.py:603
  11.2 24.8 %collective-permute-start.2 = (bf16[256,384]{1,0:T(8,128)(2,1)}, bf16[256,384]{1,0:T(8,128)(2,1)S(1)}, u32[]{:S(2)}, u32[]{:S(2)}) collective-permute-start(bf16[256,384]{1,0:T(8,128)(2,1)} %get-tuple-element.19), channel_id=1, source_target_pairs={{0,0},{1,128},{32,32},{33,160},{64,64},{65,192},{96,96},{97,224},{... | collective-permute-start | bytes 589832 | tf_op jit(solution)/shard_map/ppermute | solution.py:625
  20.3 16.1 %collective-permute-start.3 = (bf16[256,384]{1,0:T(8,128)(2,1)}, bf16[256,384]{1,0:T(8,128)(2,1)S(1)}, u32[]{:S(2)}, u32[]{:S(2)}) collective-permute-start(bf16[256,384]{1,0:T(8,128)(2,1)} %get-tuple-element.20), channel_id=1, source_target_pairs={{0,32},{1,160},{32,64},{33,192},{64,96},{65,224},{96,0},{97,128},{... | collective-permute-start | bytes 589832 | tf_op jit(solution)/shard_map/ppermute | solution.py:625
  20.3 16.0 %collective-permute-start.4 = (bf16[256,384]{1,0:T(8,128)(2,1)}, bf16[256,384]{1,0:T(8,128)(2,1)S(1)}, u32[]{:S(2)}, u32[]{:S(2)}) collective-permute-start(bf16[256,384]{1,0:T(8,128)(2,1)} %get-tuple-element.21), channel_id=1, source_target_pairs={{0,64},{1,192},{32,96},{33,224},{64,0},{65,128},{96,32},{97,160},{... | collective-permute-start | bytes 589832 | tf_op jit(solution)/shard_map/ppermute | solution.py:625
  24.7 13.4 %collective-permute-start.5 = (bf16[256,384]{1,0:T(8,128)(2,1)}, bf16[256,384]{1,0:T(8,128)(2,1)}, u32[]{:S(2)}, u32[]{:S(2)}) collective-permute-start(bf16[256,384]{1,0:T(8,128)(2,1)} %get-tuple-element.22), channel_id=1, source_target_pairs={{0,96},{1,224},{32,0},{33,128},{64,32},{65,160},{96,64},{97,192},{... | collective-permute-start | bytes 589832 | tf_op jit(solution)/shard_map/ppermute | solution.py:625
  27.6 5.9 %collective-permute-start.14 = (bf16[30,512]{1,0:T(8,128)(2,1)S(1)}, bf16[30,512]{1,0:T(8,128)(2,1)S(1)}, u32[]{:S(2)}, u32[]{:S(2)}) collective-permute-start(bf16[30,512]{1,0:T(8,128)(2,1)S(1)} %slice.273), channel_id=1, source_target_pairs={{0,8},{8,16},{16,24},{24,32},{32,40},{40,48},{48,56},{56,64},{64,7... | collective-permute-start | bytes 92168 | tf_op jit(solution)/shard_map/ppermute | solution.py:644
  34.1 43.1 %collective-permute-start.17 = (bf16[1024,512]{1,0:T(8,128)(2,1)}, bf16[1024,512]{1,0:T(8,128)(2,1)}, u32[]{:S(2)}, u32[]{:S(2)}) collective-permute-start(bf16[1024,512]{1,0:T(8,128)(2,1)} %join.1.refs_0_), channel_id=1, source_target_pairs={{0,2},{2,4},{4,6},{6,0},{1,3},{3,5},{5,7},{7,1},{8,10},{10,12},{12... | collective-permute-start | bytes 3145736 | tf_op jit(solution)/shard_map/ppermute | solution.py:636
  35.9 43.7 %collective-permute-start.18 = (bf16[1024,512]{1,0:T(8,128)(2,1)}, bf16[1024,512]{1,0:T(8,128)(2,1)}, u32[]{:S(2)}, u32[]{:S(2)}) collective-permute-start(bf16[1024,512]{1,0:T(8,128)(2,1)} %join.1.refs_0_), channel_id=1, source_target_pairs={{0,4},{2,6},{4,0},{6,2},{1,5},{3,7},{5,1},{7,3},{8,12},{10,14},{12... | collective-permute-start | bytes 3145736 | tf_op jit(solution)/shard_map/ppermute | solution.py:636
  40.1 7.3 %collective-permute-start.6 = (bf16[4,128,128]{2,1,0:T(8,128)(2,1)}, bf16[4,128,128]{2,1,0:T(8,128)(2,1)S(1)}, u32[]{:S(2)}, u32[]{:S(2)}) collective-permute-start(bf16[4,128,128]{2,1,0:T(8,128)(2,1)} %get-tuple-element.24), channel_id=1, source_target_pairs={{0,1},{1,0},{2,3},{3,2},{4,5},{5,4},{6,7},{7,6},{8,9},{9,8},{10,11... | collective-permute-start | bytes 393224 | tf_op jit(solution)/shard_map/ppermute | solution.py:603
  44.4 1.8 %collective-permute-start.15 = (f32[2,256]{1,0:T(2,128)S(1)}, f32[2,256]{1,0:T(2,128)S(1)}, u32[]{:S(2)}, u32[]{:S(2)}) collective-permute-start(f32[2,256]{1,0:T(2,128)S(1)} %pad_maximum_fusion), channel_id=1, source_target_pairs={{0,1},{1,0},{2,3},{3,2},{4,5},{5,4},{6,7},{7,6},{8,9},{9,8},{10,11... | collective-permute-start | bytes 6152 | tf_op jit(solution)/shard_map/ppermute | solution.py:603
  46.0 41.0 %collective-permute-start.19 = (bf16[1024,512]{1,0:T(8,128)(2,1)}, bf16[1024,512]{1,0:T(8,128)(2,1)S(1)}, u32[]{:S(2)}, u32[]{:S(2)}) collective-permute-start(bf16[1024,512]{1,0:T(8,128)(2,1)} %join.1.refs_0_), channel_id=1, source_target_pairs={{0,6},{2,0},{4,2},{6,4},{1,7},{3,1},{5,3},{7,5},{8,14},{10,8},{12,... | collective-permute-start | bytes 3145736 | tf_op jit(solution)/shard_map/ppermute | solution.py:636
  46.2 33.4 %collective-permute-start.8 = (bf16[4,256,256]{2,1,0:T(8,128)(2,1)}, bf16[4,256,256]{2,1,0:T(8,128)(2,1)}, u32[]{:S(2)}, u32[]{:S(2)}) collective-permute-start(bf16[4,256,256]{2,1,0:T(8,128)(2,1)} %get-tuple-element.25.kv_a), channel_id=1, source_target_pairs={{0,8},{8,16},{16,24},{24,0},{1,9},{9,17},{17,25},{25,1},{2,10},{10... | collective-permute-start | bytes 1572872 | tf_op jit(solution)/shard_map/ppermute | solution.py:632
  47.4 32.7 %collective-permute-start.10 = (bf16[4,256,256]{2,1,0:T(8,128)(2,1)}, bf16[4,256,256]{2,1,0:T(8,128)(2,1)}, u32[]{:S(2)}, u32[]{:S(2)}) collective-permute-start(bf16[4,256,256]{2,1,0:T(8,128)(2,1)} %get-tuple-element.25.kv_a), channel_id=1, source_target_pairs={{0,24},{8,0},{16,8},{24,16},{1,25},{9,1},{17,9},{25,17},{2,26},{10... | collective-permute-start | bytes 1572872 | tf_op jit(solution)/shard_map/ppermute | solution.py:632
  77.2 9.9 %collective-permute-start.12 = (bf16[4,256,256]{2,1,0:T(8,128)(2,1)}, bf16[4,256,256]{2,1,0:T(8,128)(2,1)}, u32[]{:S(2)}, u32[]{:S(2)}) collective-permute-start(bf16[4,256,256]{2,1,0:T(8,128)(2,1)} %get-tuple-element.25.kv_a), channel_id=1, source_target_pairs={{0,16},{8,24},{16,0},{24,8},{1,17},{9,25},{17,1},{25,9},{2,18},{10... | collective-permute-start | bytes 1572872 | tf_op jit(solution)/shard_map/ppermute | solution.py:632
  79.6 8.0 %collective-permute-start.7 = (bf16[4,256,256]{2,1,0:T(8,128)(2,1)}, bf16[4,256,256]{2,1,0:T(8,128)(2,1)}, u32[]{:S(2)}, u32[]{:S(2)}) collective-permute-start(bf16[4,256,256]{2,1,0:T(8,128)(2,1)} %get-tuple-element.25.kv_a), channel_id=1, source_target_pairs={{0,1},{1,0},{2,3},{3,2},{4,5},{5,4},{6,7},{7,6},{8,9},{9,8},{10,11... | collective-permute-start | bytes 1572872 | tf_op jit(solution)/shard_map/ppermute | solution.py:603
  79.6 8.1 %collective-permute-start.9 = (bf16[4,256,256]{2,1,0:T(8,128)(2,1)}, bf16[4,256,256]{2,1,0:T(8,128)(2,1)}, u32[]{:S(2)}, u32[]{:S(2)}) collective-permute-start(bf16[4,256,256]{2,1,0:T(8,128)(2,1)} %collective-permute-done.8.kv_a), channel_id=1, source_target_pairs={{0,1},{1,0},{2,3},{3,2},{4,5},{5,4},{6,7},{7,6},{8,9},{9,8},{10,11... | collective-permute-start | bytes 1572872 | tf_op jit(solution)/shard_map/ppermute | solution.py:603
  80.1 8.0 %collective-permute-start.11 = (bf16[4,256,256]{2,1,0:T(8,128)(2,1)}, bf16[4,256,256]{2,1,0:T(8,128)(2,1)}, u32[]{:S(2)}, u32[]{:S(2)}) collective-permute-start(bf16[4,256,256]{2,1,0:T(8,128)(2,1)} %collective-permute-done.10.kv_c), channel_id=1, source_target_pairs={{0,1},{1,0},{2,3},{3,2},{4,5},{5,4},{6,7},{7,6},{8,9},{9,8},{10,11... | collective-permute-start | bytes 1572872 | tf_op jit(solution)/shard_map/ppermute | solution.py:603
  87.0 16.8 %collective-permute-start.13 = (bf16[4,256,256]{2,1,0:T(8,128)(2,1)}, bf16[4,256,256]{2,1,0:T(8,128)(2,1)}, u32[]{:S(2)}, u32[]{:S(2)}) collective-permute-start(bf16[4,256,256]{2,1,0:T(8,128)(2,1)} %collective-permute-done.12.kv_a), channel_id=1, source_target_pairs={{0,1},{1,0},{2,3},{3,2},{4,5},{5,4},{6,7},{7,6},{8,9},{9,8},{10,11... | collective-permute-start | bytes 1572872 | tf_op jit(solution)/shard_map/ppermute | solution.py:603
  87.0 43.5 %collective-permute-start.20 = (bf16[1024,512]{1,0:T(8,128)(2,1)}, bf16[1024,512]{1,0:T(8,128)(2,1)}, u32[]{:S(2)}, u32[]{:S(2)}) collective-permute-start(bf16[1024,512]{1,0:T(8,128)(2,1)} %join.1.refs_0_), channel_id=1, source_target_pairs={{0,1},{1,0},{2,3},{3,2},{4,5},{5,4},{6,7},{7,6},{8,9},{9,8},{10,11... | collective-permute-start | bytes 3145736 | tf_op jit(solution)/shard_map/ppermute | solution.py:603
  87.6 43.0 %collective-permute-start.21 = (bf16[1024,512]{1,0:T(8,128)(2,1)}, bf16[1024,512]{1,0:T(8,128)(2,1)}, u32[]{:S(2)}, u32[]{:S(2)}) collective-permute-start(bf16[1024,512]{1,0:T(8,128)(2,1)} %collective-permute-done.17.refs_1_), channel_id=1, source_target_pairs={{0,1},{1,0},{2,3},{3,2},{4,5},{5,4},{6,7},{7,6},{8,9},{9,8},{10,11... | collective-permute-start | bytes 3145736 | tf_op jit(solution)/shard_map/ppermute | solution.py:603
  87.7 42.8 %collective-permute-start.22 = (bf16[1024,512]{1,0:T(8,128)(2,1)}, bf16[1024,512]{1,0:T(8,128)(2,1)}, u32[]{:S(2)}, u32[]{:S(2)}) collective-permute-start(bf16[1024,512]{1,0:T(8,128)(2,1)} %collective-permute-done.18.refs_2_), channel_id=1, source_target_pairs={{0,1},{1,0},{2,3},{3,2},{4,5},{5,4},{6,7},{7,6},{8,9},{9,8},{10,11... | collective-permute-start | bytes 3145736 | tf_op jit(solution)/shard_map/ppermute | solution.py:603
  88.2 42.4 %collective-permute-start.23 = (bf16[1024,512]{1,0:T(8,128)(2,1)S(1)}, bf16[1024,512]{1,0:T(8,128)(2,1)}, u32[]{:S(2)}, u32[]{:S(2)}) collective-permute-start(bf16[1024,512]{1,0:T(8,128)(2,1)S(1)} %collective-permute-done.19.refs_3_), channel_id=1, source_target_pairs={{0,1},{1,0},{2,3},{3,2},{4,5},{5,4},{6,7},{7,6},{8,9},{9,8},{10,11... | collective-permute-start | bytes 3145736 | tf_op jit(solution)/shard_map/ppermute | solution.py:603
  109.9 29.5 %all-to-all-start = ((bf16[8,136,128]{2,1,0:T(8,128)(2,1)}), bf16[8,136,128]{2,1,0:T(8,128)(2,1)S(1)}, u32[]{:S(2)}, u32[]{:S(2)}) async-start(bf16[8,136,128]{2,1,0:T(8,128)(2,1)} %attend_last.1), calls=%async_computation | async-start | bytes 557056 | tf_op jit(solution)/shard_map/all_to_all | solution.py:675
  139.5 5.2 %collective-permute-start.24 = (f32[4,2,128]{2,0,1:T(4,128)S(1)}, f32[4,2,128]{2,0,1:T(4,128)S(1)}, u32[]{:S(2)}, u32[]{:S(2)}) collective-permute-start(f32[4,2,128]{2,0,1:T(4,128)S(1)} %bitcast.102), channel_id=1, source_target_pairs={{0,1},{1,0},{2,3},{3,2},{4,5},{5,4},{6,7},{7,6},{8,9},{9,8},{10,11... | collective-permute-start | bytes 12296 | tf_op jit(solution)/shard_map/ppermute | solution.py:603
  (18 other events, 167.1 us)
